TPU v7x, 32 devices: a whole 2x2x4 slice. The times are simulated.
32 devices in a mesh: ra: 4 (over z), cb: 4 (over y, x), dp: 2 (over core).
Axes of the slice: x: 2, y: 2, z: 4, core: 2. Of those that a mesh axis runs over, the one named last changes fastest.
Arguments:
- tokens: bfloat16 [2, 512, 4096], P('dp', None, 'ra'), may hold values from -80 to 80
- pre_gain: float32 [4096], P('ra'), may hold values from 0.1 to 1.9
- w_gate: bfloat16 [4096, 11264], P('ra', 'cb'), may hold values from -0.09375 to 0.09375
- w_up: bfloat16 [4096, 11264], P('ra', 'cb'), may hold values from -0.09375 to 0.09375
- conv_gate: float32 [3, 11264], P(None, 'cb'), may hold values from -3.5 to 3.5
- conv_up: float32 [3, 11264], P(None, 'cb'), may hold values from -3.5 to 3.5
- w_down: bfloat16 [11264, 4096], P('cb', 'ra'), may hold values from -2 to 2
- post_gain: float32 [4096], P('ra'), may hold values from 0.1 to 1.9
Outputs:
- mixed: bfloat16 [2, 512, 4096], P('dp', None, 'ra')
All inputs are finite; a program needn't handle non-finite values.
Results may differ from a plain program's by a relative error of at most 0.0064.
Values may be sent and summed in bfloat16 or wider, within the bound.
A program may use at most 128 MiB of HBM per device.

v0:
```python
import jax
import jax.numpy as jnp
from jax import lax
from jax.sharding import PartitionSpec as P

epsilon = 1e-06
residual_scale = 0.125


def convolve(field, tap_weights):
    zero_col = jnp.zeros((field.shape[0], 1), jnp.float32)
    before = jnp.concatenate([zero_col, field[:, :-1]], axis=1)
    later_cols = jnp.concatenate([field[:, 1:], zero_col], axis=1)
    return (
        tap_weights[0][:, None] * before
        + tap_weights[1][:, None] * field
        + tap_weights[2][:, None] * later_cols
    )


def local(tokens, pre_gain, w_gate, w_up, conv_gate, conv_up, w_down, post_gain):
    ra_count = lax.axis_size("ra")
    dim_full = tokens.shape[2] * ra_count
    values = tokens[0].astype(jnp.float32)
    local_sq = jnp.sum(values * values, axis=1)
    total_sq = lax.psum(local_sq, "ra")
    in_scale = lax.rsqrt(total_sq / dim_full + epsilon)
    weighted = (values * pre_gain).astype(jnp.bfloat16)
    gate_cols, up_cols = (
        lax.all_to_all(w_gate, "ra", split_axis=1, concat_axis=0, tiled=True),
        lax.all_to_all(w_up, "ra", split_axis=1, concat_axis=0, tiled=True),
    )
    own_units = gate_cols.shape[1]
    piece = lax.all_gather(weighted, "ra", axis=1, tiled=True)
    dims = (((0,), (1,)), ((), ()))
    gate_sum = lax.dot_general(gate_cols, piece, dims, preferred_element_type=jnp.float32)
    up_sum = lax.dot_general(up_cols, piece, dims, preferred_element_type=jnp.float32)
    offset_units = lax.axis_index("ra") * own_units
    taps_gate = lax.dynamic_slice_in_dim(conv_gate, offset_units, own_units, 1)
    taps_up = lax.dynamic_slice_in_dim(conv_up, offset_units, own_units, 1)
    gate_lin = gate_sum * in_scale[None, :]
    up_lin = up_sum * in_scale[None, :]
    hidden = (
        jax.nn.gelu(convolve(gate_lin, taps_gate), approximate=True) * convolve(up_lin, taps_up)
    ).astype(jnp.bfloat16)
    partial_value = lax.dot_general(
        lax.all_gather(hidden, "ra", axis=0, tiled=True),
        w_down,
        (((0,), (0,)), ((), ())),
        preferred_element_type=jnp.float32,
    )
    branch = lax.psum(partial_value, "cb")
    post_sq = lax.psum(jnp.sum(branch * branch, axis=1), "ra")
    post_scale = lax.rsqrt(post_sq / dim_full + epsilon)
    mixed = residual_scale * values + branch * post_scale[:, None] * post_gain
    return mixed.astype(jnp.bfloat16)[None]


def solution(mesh):
    in_specs = (
        P("dp", None, "ra"),
        P("ra"),
        P("ra", "cb"),
        P("ra", "cb"),
        P(None, "cb"),
        P(None, "cb"),
        P("cb", "ra"),
        P("ra"),
    )
    out_specs = P("dp", None, "ra")
    return jax.shard_map(local, mesh=mesh, in_specs=in_specs, out_specs=out_specs, check_vma=False)
```

profile of v0, /device:TPU:0, one launch (start us, length us, event | category | flops | bytes accessed | tf_op | source)
XLA Modules:
  0.0 532.4 jit_solution(12061142635943834656)
XLA Ops:
  6.5 8.3 %copy.11 = bf16[1024,2816]{0,1:T(8,128)(2,1)} copy(bf16[1024,2816]{1,0:T(8,128)(2,1)} %param.11) | data formatting | bytes 11534336 | tf_op args[3]
  14.8 6.3 %all-to-all-start.1 = ((bf16[1024,4,704]{0,2,1:T(8,128)(2,1)}), bf16[1024,4,704]{0,2,1:T(8,128)(2,1)}, u32[]{:S(2)}, u32[]{:S(2)}) async-start(bf16[1024,4,704]{0,2,1:T(8,128)(2,1)} %bitcast.26), calls=%async_computation.1 | async-start | bytes 11534336 | tf_op jit(solution)/shard_map/all_to_all | solution.py:31
  21.1 8.3 %copy.9 = bf16[1024,2816]{0,1:T(8,128)(2,1)} copy(bf16[1024,2816]{1,0:T(8,128)(2,1)} %param.10) | data formatting | bytes 11534336 | tf_op args[2]
  29.5 119.1 %all-to-all-done.1 = bf16[1024,4,704]{0,2,1:T(8,128)(2,1)} async-done(((bf16[1024,4,704]{0,2,1:T(8,128)(2,1)}), bf16[1024,4,704]{0,2,1:T(8,128)(2,1)}, u32[]{:S(2)}, u32[]{:S(2)}) %all-to-all-start.1) | async-done | bytes 5767200 | tf_op jit(solution)/shard_map/all_to_all | solution.py:31
  148.6 0.0 copy-start.2
  148.6 0.0 copy-start.3
  148.6 5.3 all-to-all-start
  153.9 0.0 all-gather.3.cloned.1.call-start
  154.0 0.0 copy-done.2
  154.0 0.0 copy-done.3
  154.0 1.3 fusion.3
  155.2 0.0 all-gather.3.cloned.1.call-update
  155.3 0.0 all-gather.5.cloned.1.call-start
  155.3 1.0 dynamic-slice_reduce_fusion.2
  156.3 163.7 %psum.21 = f32[512]{0:T(512)S(1)} all-reduce(f32[512]{0:T(512)S(1)} %get-tuple-element.15), channel_id=1, replica_groups=mesh['ra'=4,'cb'=4,'dp'=2] {'ra'}, use_global_device_ids=true, to_apply=%region_1.0 | all-reduce | flops 512 | bytes 4096 | tf_op jit(solution)/shard_map/psum | solution.py:26
  320.0 6.1 %copy.14 = bf16[4,88,8,1024]{3,2,0,1:T(8,128)(2,1)} copy(bf16[4,88,8,1024]{3,2,1,0:T(8,128)(2,1)} %bitcast.11) | data formatting | bytes 11534336 | tf_op jit(solution)/shard_map/all_to_all | solution.py:31
  326.1 22.0 %all-to-all-done = bf16[1024,4,704]{0,2,1:T(8,128)(2,1)} async-done(((bf16[1024,4,704]{0,2,1:T(8,128)(2,1)}), bf16[1024,4,704]{0,2,1:T(8,128)(2,1)}, u32[]{:S(2)}, u32[]{:S(2)}) %all-to-all-start) | async-done | bytes 5767200 | tf_op jit(solution)/shard_map/all_to_all | solution.py:30
  348.1 6.1 %copy.13 = bf16[4,88,8,1024]{3,2,0,1:T(8,128)(2,1)} copy(bf16[4,88,8,1024]{3,2,1,0:T(8,128)(2,1)} %bitcast.9) | data formatting | bytes 11534336 | tf_op jit(solution)/shard_map/all_to_all | solution.py:30
  354.3 0.0 all-gather.3.cloned.1.call-done
  354.3 0.0 copy-start.1
  354.3 0.0 copy-start.5
  354.3 6.6 %fusion.4 = f32[704,512]{1,0:T(8,128)S(1)} fusion(bf16[512,4096]{1,0:T(8,128)(2,1)} %all-gather.3.cloned.1.call-done, bf16[4096,704]{0,1:T(8,128)(2,1)} %bitcast.27, f32[512]{0:T(512)S(1)} %add_rsqrt_fusion.1), kind=kOutput, calls=%fused_computation.10 | convolution fusion | flops 2953150464 | bytes 11405312 | tf_op jit(solution)/shard_map/dot_general | solution.py:37
  360.9 0.0 copy-done.1
  360.9 0.1 copy-done.5
  361.0 3.2 fusion.5
  364.2 1.0 fusion.16
  365.2 2.8 fusion.14
  368.0 0.0 all-gather.5.cloned.1.call-update
  368.0 0.0 all-reduce.6.cloned.1.call-start
  368.1 66.4 %all-gather.5.cloned.1.call-done = bf16[2816,512]{1,0:T(8,128)(2,1)} async-done(((bf16[704,512]{1,0:T(8,128)(2,1)}), bf16[2816,512]{1,0:T(8,128)(2,1)}) %all-gather.5.cloned.1.call-update) | async-done | bytes 2883600 | tf_op jit(solution)/shard_map/all_gather | solution.py:47
  434.5 8.0 %fusion.18 = f32[512,1024]{1,0:T(8,128)} fusion(bf16[2816,512]{1,0:T(8,128)(2,1)} %all-gather.5.cloned.1.call-done, bf16[2816,1024]{1,0:T(8,128)(2,1)} %param.14), kind=kOutput, calls=%fused_computation.33 | convolution fusion | flops 2952790016 | bytes 10747904 | tf_op jit(solution)/shard_map/dot_general | solution.py:46
  442.5 0.0 all-reduce.6.cloned.1.call-update
  442.5 0.0 copy-start.4
  442.5 68.3 %all-reduce.6.cloned.1.call-done = f32[512,1024]{1,0:T(8,128)} async-done(((f32[512,1024]{1,0:T(8,128)}), f32[512,1024]{1,0:T(8,128)}) %all-reduce.6.cloned.1.call-update) | async-done | bytes 2097168 | tf_op jit(solution)/shard_map/psum | solution.py:52
  510.8 0.0 copy-start
  510.8 2.0 multiply_reduce_fusion
  512.8 11.7 %psum.23 = f32[512]{0:T(512)S(1)} all-reduce(f32[512]{0:T(512)S(1)} %multiply_reduce_fusion), channel_id=1, replica_groups=mesh['ra'=4,'cb'=4,'dp'=2] {'ra'}, use_global_device_ids=true, to_apply=%region_4.0 | all-reduce | flops 512 | bytes 4096 | tf_op jit(solution)/shard_map/psum | solution.py:53
  524.5 0.0 copy-done.4
  524.5 0.0 copy-done
  524.5 1.4 fusion.15
  (2 shorter events, 0.0 us)
Async XLA Ops:
  14.8 133.8 %all-to-all-start.1 = ((bf16[1024,4,704]{0,2,1:T(8,128)(2,1)}), bf16[1024,4,704]{0,2,1:T(8,128)(2,1)}, u32[]{:S(2)}, u32[]{:S(2)}) async-start(bf16[1024,4,704]{0,2,1:T(8,128)(2,1)} %bitcast.26), calls=%async_computation.1 | async-start | bytes 11534336 | tf_op jit(solution)/shard_map/all_to_all | solution.py:31
  148.6 5.3 %copy-start.2 = (bf16[1,512,1024]{2,1,0:T(8,128)(2,1)S(1)}, bf16[1,512,1024]{2,1,0:T(8,128)(2,1)}, u32[]{:S(2)}) copy-start(bf16[1,512,1024]{2,1,0:T(8,128)(2,1)} %param.8) | copy-start | bytes 3145732
  148.6 5.4 %copy-start.3 = (f32[1024]{0:T(1024)S(1)}, f32[1024]{0:T(1024)}, u32[]{:S(2)}) copy-start(f32[1024]{0:T(1024)} %param.9) | copy-start | bytes 12292
  148.6 199.5 %all-to-all-start = ((bf16[1024,4,704]{0,2,1:T(8,128)(2,1)}), bf16[1024,4,704]{0,2,1:T(8,128)(2,1)}, u32[]{:S(2)}, u32[]{:S(2)}) async-start(bf16[1024,4,704]{0,2,1:T(8,128)(2,1)} %bitcast.25), calls=%async_computation | async-start | bytes 11534336 | tf_op jit(solution)/shard_map/all_to_all | solution.py:30
  153.9 200.4 %all-gather.3.cloned.1.call-start = ((), (), s32[]{:S(2)}) async-start(), calls=%async_computation.2 | async-start | bytes 5242880 | tf_op jit(solution)/shard_map/all_gather | solution.py:34
  155.3 279.2 %all-gather.5.cloned.1.call-start = ((), (), s32[]{:S(2)}) async-start(), calls=%async_computation.3 | async-start | bytes 3604480 | tf_op jit(solution)/shard_map/all_gather | solution.py:47
  354.3 6.6 %copy-start.1 = (bf16[4,88,8,1024]{3,2,0,1:T(8,128)(2,1)S(1)}, bf16[4,88,8,1024]{3,2,0,1:T(8,128)(2,1)}, u32[]{:S(2)}) copy-start(bf16[4,88,8,1024]{3,2,0,1:T(8,128)(2,1)} %copy.13) | copy-start | bytes 17301508
  354.3 6.8 %copy-start.5 = (bf16[512,4096]{1,0:T(8,128)(2,1)S(1)}, bf16[512,4096]{1,0:T(8,128)(2,1)}, u32[]{:S(2)}) copy-start(bf16[512,4096]{1,0:T(8,128)(2,1)} %all-gather.3.cloned.1.call-done) | copy-start | bytes 12582916
  368.0 142.8 %all-reduce.6.cloned.1.call-start = ((), (), s32[]{:S(2)}) async-start(), calls=%async_computation.4 | async-start | bytes 4194304 | tf_op jit(solution)/shard_map/psum | solution.py:52
  442.5 82.0 %copy-start.4 = (f32[1024]{0:T(1024)S(1)}, f32[1024]{0:T(1024)}, u32[]{:S(2)}) copy-start(f32[1024]{0:T(1024)} %param.15) | copy-start | bytes 12292
  510.8 13.7 %copy-start = (f32[512,1024]{1,0:T(8,128)S(1)}, f32[512,1024]{1,0:T(8,128)}, u32[]{:S(2)}) copy-start(f32[512,1024]{1,0:T(8,128)} %all-reduce.6.cloned.1.call-done) | copy-start | bytes 6291460
Sparse Core Ops, SparseCore 0:
  156.3 164.8 all-gather.2
  368.2 66.2 all-gather.4
  442.6 68.1 all-reduce.5
where the time goes:
time: 533 us; the launch traced here: 532 us
  waiting for transfers between devices  276 us (52%)
  blocking collectives  175 us (33%)
  local copies, waits for them, and re-layouts  31 us (6%)
  matrix products  17.8 us (3%)
  between operations  13.2 us (2%)
  starting transfers between devices  11.8 us (2%)
  other arithmetic  7.39 us (1%)
    psum x1, blocking collectives, local(): total_sq = lax.psum(local_sq, 'ra')  164 us
    all_to_all x1, waiting for transfers between devices, local(): lax.all_to_all(w_up, 'ra', split_axis=1, concat_axis=0, tiled=True)  119 us
    psum x1, waiting for transfers between devices, local(): branch = lax.psum(partial_value, 'cb')  68.3 us
    all_gather x1, waiting for transfers between devices, local(): lax.all_gather(hidden, 'ra', axis=0, tiled=True)  66.4 us
    all_to_all x1, waiting for transfers between devices, local(): lax.all_to_all(w_gate, 'ra', split_axis=1, concat_axis=0, tiled=True)  22 us
    unnamed x14, local copies, waits for them, and re-layouts  16.7 us
    psum x1, blocking collectives, local(): post_sq = lax.psum(jnp.sum(branch * branch, axis=1), 'ra')  11.7 us
  transfers between devices with their start and end apart: 5, of which 4 were waited for; matrix products, arithmetic and copies ran while one was open for 4% of the time, Pallas kernels for 0%

commit v1 on v0

--- a/solution.py
+++ b/solution.py
@@ -49,7 +49,10 @@
         (((0,), (0,)), ((), ())),
         preferred_element_type=jnp.float32,
     )
-    branch = lax.psum(partial_value, "cb")
+    size, branch = (lax.axis_size("cb"), partial_value)
+    for stride in [1 << k for k in range(size.bit_length() - 1)]:
+        swap = [(i, i ^ stride) for i in range(size)]
+        branch = branch + lax.ppermute(branch, "cb", swap)
     post_sq = lax.psum(jnp.sum(branch * branch, axis=1), "ra")
     post_scale = lax.rsqrt(post_sq / dim_full + epsilon)
     mixed = residual_scale * values + branch * post_scale[:, None] * post_gain

time: 533 us -> 554 us (1.039)
  waiting for transfers between devices: 276 us -> 298 us
    ppermute x0 -> x2, waiting for transfers between devices: none -> 90.6 us  [local(): branch = branch + lax.ppermute(branch, 'cb', swap)]
    psum x1 -> x0, waiting for transfers between devices: 68.3 us -> none  [local(): branch = lax.psum(partial_value, 'cb')]
    unnamed x14 -> x12, local copies, waits for them, and re-layouts: 16.7 us -> 16.7 us
  transfers between devices with their start and end apart: 5 -> 6, of which waited for: 4 -> 5; matrix products, arithmetic and copies ran while one was open for 4% -> 4% of each run, Pallas kernels for 0% -> 0%
where the time goes in v1:
time: 554 us; the launch traced here: 553 us
  waiting for transfers between devices  298 us (54%)
  blocking collectives  174 us (31%)
  local copies, waits for them, and re-layouts  31 us (6%)
  matrix products  15.9 us (3%)
  starting transfers between devices  14.8 us (3%)
  between operations  13.5 us (2%)
  other arithmetic  6.29 us (1%)
    psum x1, blocking collectives, local(): total_sq = lax.psum(local_sq, 'ra')  164 us
    all_to_all x1, waiting for transfers between devices, local(): lax.all_to_all(w_up, 'ra', split_axis=1, concat_axis=0, tiled=True)  119 us
    ppermute x2, waiting for transfers between devices, local(): branch = branch + lax.ppermute(branch, 'cb', swap)  90.6 us
    all_gather x1, waiting for transfers between devices, local(): lax.all_gather(hidden, 'ra', axis=0, tiled=True)  66.4 us
    all_to_all x1, waiting for transfers between devices, local(): lax.all_to_all(w_gate, 'ra', split_axis=1, concat_axis=0, tiled=True)  22 us
    unnamed x12, local copies, waits for them, and re-layouts  16.7 us
  transfers between devices with their start and end apart: 6, of which 5 were waited for; matrix products, arithmetic and copies ran while one was open for 4% of the time, Pallas kernels for 0%

profile of v1, /device:TPU:0, one launch (start us, length us, event | category | flops | bytes accessed | tf_op | source)
XLA Modules:
  0.0 553.2 jit_solution(729006522425659918)
XLA Ops:
  6.5 8.3 %copy.11 = bf16[1024,2816]{0,1:T(8,128)(2,1)} copy(bf16[1024,2816]{1,0:T(8,128)(2,1)} %param.11) | data formatting | bytes 11534336 | tf_op args[3]
  14.8 6.3 %all-to-all-start.1 = ((bf16[1024,4,704]{0,2,1:T(8,128)(2,1)}), bf16[1024,4,704]{0,2,1:T(8,128)(2,1)}, u32[]{:S(2)}, u32[]{:S(2)}) async-start(bf16[1024,4,704]{0,2,1:T(8,128)(2,1)} %bitcast.26), calls=%async_computation.1 | async-start | bytes 11534336 | tf_op jit(solution)/shard_map/all_to_all | solution.py:31
  21.1 8.3 %copy.9 = bf16[1024,2816]{0,1:T(8,128)(2,1)} copy(bf16[1024,2816]{1,0:T(8,128)(2,1)} %param.10) | data formatting | bytes 11534336 | tf_op args[2]
  29.5 119.1 %all-to-all-done.1 = bf16[1024,4,704]{0,2,1:T(8,128)(2,1)} async-done(((bf16[1024,4,704]{0,2,1:T(8,128)(2,1)}), bf16[1024,4,704]{0,2,1:T(8,128)(2,1)}, u32[]{:S(2)}, u32[]{:S(2)}) %all-to-all-start.1) | async-done | bytes 5767200 | tf_op jit(solution)/shard_map/all_to_all | solution.py:31
  148.6 0.0 copy-start.1
  148.6 0.0 copy-start.2
  148.6 5.3 all-to-all-start
  153.9 0.0 all-gather.3.cloned.1.call-start
  154.0 0.0 copy-done.1
  154.0 0.0 copy-done.2
  154.0 1.3 fusion.3
  155.2 0.0 all-gather.3.cloned.1.call-update
  155.3 0.0 all-gather.5.cloned.1.call-start
  155.3 1.0 dynamic-slice_reduce_fusion.2
  156.3 163.7 %psum.14 = f32[512]{0:T(512)S(1)} all-reduce(f32[512]{0:T(512)S(1)} %get-tuple-element.17), channel_id=1, replica_groups=mesh['ra'=4,'cb'=4,'dp'=2] {'ra'}, use_global_device_ids=true, to_apply=%region_1.0 | all-reduce | flops 512 | bytes 4096 | tf_op jit(solution)/shard_map/psum | solution.py:26
  320.0 6.1 %copy.14 = bf16[4,88,8,1024]{3,2,0,1:T(8,128)(2,1)} copy(bf16[4,88,8,1024]{3,2,1,0:T(8,128)(2,1)} %bitcast.11) | data formatting | bytes 11534336 | tf_op jit(solution)/shard_map/all_to_all | solution.py:31
  326.1 22.0 %all-to-all-done = bf16[1024,4,704]{0,2,1:T(8,128)(2,1)} async-done(((bf16[1024,4,704]{0,2,1:T(8,128)(2,1)}), bf16[1024,4,704]{0,2,1:T(8,128)(2,1)}, u32[]{:S(2)}, u32[]{:S(2)}) %all-to-all-start) | async-done | bytes 5767200 | tf_op jit(solution)/shard_map/all_to_all | solution.py:30
  348.1 6.1 %copy.13 = bf16[4,88,8,1024]{3,2,0,1:T(8,128)(2,1)} copy(bf16[4,88,8,1024]{3,2,1,0:T(8,128)(2,1)} %bitcast.9) | data formatting | bytes 11534336 | tf_op jit(solution)/shard_map/all_to_all | solution.py:30
  354.3 0.0 all-gather.3.cloned.1.call-done
  354.3 0.0 copy-start
  354.3 0.0 copy-start.4
  354.3 6.6 %fusion.4 = f32[704,512]{1,0:T(8,128)S(1)} fusion(bf16[512,4096]{1,0:T(8,128)(2,1)} %all-gather.3.cloned.1.call-done, bf16[4096,704]{0,1:T(8,128)(2,1)} %bitcast.27, f32[512]{0:T(512)S(1)} %add_rsqrt_fusion.1), kind=kOutput, calls=%fused_computation.10 | convolution fusion | flops 2953150464 | bytes 11405312 | tf_op jit(solution)/shard_map/dot_general | solution.py:37
  360.9 0.0 copy-done
  360.9 0.1 copy-done.4
  361.0 3.2 fusion.5
  364.2 1.0 fusion.16
  365.2 2.8 fusion.14
  368.0 0.0 all-gather.5.cloned.1.call-update
  368.0 66.4 %all-gather.5.cloned.1.call-done = bf16[2816,512]{1,0:T(8,128)(2,1)} async-done(((bf16[704,512]{1,0:T(8,128)(2,1)}), bf16[2816,512]{1,0:T(8,128)(2,1)}) %all-gather.5.cloned.1.call-update) | async-done | bytes 2883600 | tf_op jit(solution)/shard_map/all_gather | solution.py:47
  434.5 6.1 %fusion.18 = f32[512,1024]{1,0:T(8,128)S(1)} fusion(bf16[2816,512]{1,0:T(8,128)(2,1)} %all-gather.5.cloned.1.call-done, bf16[2816,1024]{1,0:T(8,128)(2,1)} %param.14), kind=kOutput, calls=%fused_computation.33 | convolution fusion | flops 2952790016 | bytes 10747904 | tf_op jit(solution)/shard_map/dot_general | solution.py:46
  440.6 1.5 collective-permute-start
  442.1 45.7 %collective-permute-done = f32[512,1024]{1,0:T(8,128)S(1)} collective-permute-done((f32[512,1024]{1,0:T(8,128)S(1)}, f32[512,1024]{1,0:T(8,128)S(1)}, u32[]{:S(2)}, u32[]{:S(2)}) %collective-permute-start) | collective-permute-done | bytes 2097184 | tf_op jit(solution)/shard_map/ppermute | solution.py:55
  487.8 0.6 add.61
  488.4 0.0 copy-start.3
  488.4 1.5 collective-permute-start.1
  489.9 44.9 %collective-permute-done.1 = f32[512,1024]{1,0:T(8,128)S(1)} collective-permute-done((f32[512,1024]{1,0:T(8,128)S(1)}, f32[512,1024]{1,0:T(8,128)S(1)}, u32[]{:S(2)}, u32[]{:S(2)}) %collective-permute-start.1) | collective-permute-done | bytes 2097184 | tf_op jit(solution)/shard_map/ppermute | solution.py:55
  534.8 0.3 multiply_reduce_fusion
  535.1 9.9 %psum.15 = f32[512]{0:T(512)S(1)} all-reduce(f32[512]{0:T(512)S(1)} %get-tuple-element.11), channel_id=1, replica_groups=mesh['ra'=4,'cb'=4,'dp'=2] {'ra'}, use_global_device_ids=true, to_apply=%region_3.0 | all-reduce | flops 512 | bytes 4096 | tf_op jit(solution)/shard_map/psum | solution.py:56
  545.0 0.0 copy-done.3
  545.0 1.4 fusion.15
  (2 shorter events, 0.0 us)
Async XLA Ops:
  14.8 133.8 %all-to-all-start.1 = ((bf16[1024,4,704]{0,2,1:T(8,128)(2,1)}), bf16[1024,4,704]{0,2,1:T(8,128)(2,1)}, u32[]{:S(2)}, u32[]{:S(2)}) async-start(bf16[1024,4,704]{0,2,1:T(8,128)(2,1)} %bitcast.26), calls=%async_computation.1 | async-start | bytes 11534336 | tf_op jit(solution)/shard_map/all_to_all | solution.py:31
  148.6 5.3 copy-start.1
  148.6 5.4 copy-start.2
  148.6 199.5 %all-to-all-start = ((bf16[1024,4,704]{0,2,1:T(8,128)(2,1)}), bf16[1024,4,704]{0,2,1:T(8,128)(2,1)}, u32[]{:S(2)}, u32[]{:S(2)}) async-start(bf16[1024,4,704]{0,2,1:T(8,128)(2,1)} %bitcast.25), calls=%async_computation | async-start | bytes 11534336 | tf_op jit(solution)/shard_map/all_to_all | solution.py:30
  153.9 200.4 %all-gather.3.cloned.1.call-start = ((), (), s32[]{:S(2)}) async-start(), calls=%async_computation.2 | async-start | bytes 5242880 | tf_op jit(solution)/shard_map/all_gather | solution.py:34
  155.3 279.2 %all-gather.5.cloned.1.call-start = ((), (), s32[]{:S(2)}) async-start(), calls=%async_computation.3 | async-start | bytes 3604480 | tf_op jit(solution)/shard_map/all_gather | solution.py:47
  354.3 6.6 %copy-start = (bf16[4,88,8,1024]{3,2,0,1:T(8,128)(2,1)S(1)}, bf16[4,88,8,1024]{3,2,0,1:T(8,128)(2,1)}, u32[]{:S(2)}) copy-start(bf16[4,88,8,1024]{3,2,0,1:T(8,128)(2,1)} %copy.13) | copy-start | bytes 17301508
  354.3 6.8 %copy-start.4 = (bf16[512,4096]{1,0:T(8,128)(2,1)S(1)}, bf16[512,4096]{1,0:T(8,128)(2,1)}, u32[]{:S(2)}) copy-start(bf16[512,4096]{1,0:T(8,128)(2,1)} %all-gather.3.cloned.1.call-done) | copy-start | bytes 12582916
  440.6 47.3 %collective-permute-start = (f32[512,1024]{1,0:T(8,128)S(1)}, f32[512,1024]{1,0:T(8,128)S(1)}, u32[]{:S(2)}, u32[]{:S(2)}) collective-permute-start(f32[512,1024]{1,0:T(8,128)S(1)} %fusion.18), channel_id=1, source_target_pairs={{0,2},{2,0},{4,6},{6,4},{1,3},{3,1},{5,7},{7,5},{8,10},{10,8},{12,... | collective-permute-start | bytes 6291464 | tf_op jit(solution)/shard_map/ppermute | solution.py:55
  488.4 56.6 %copy-start.3 = (f32[1024]{0:T(1024)S(1)}, f32[1024]{0:T(1024)}, u32[]{:S(2)}) copy-start(f32[1024]{0:T(1024)} %param.15) | copy-start | bytes 12292
  488.4 46.4 %collective-permute-start.1 = (f32[512,1024]{1,0:T(8,128)S(1)}, f32[512,1024]{1,0:T(8,128)S(1)}, u32[]{:S(2)}, u32[]{:S(2)}) collective-permute-start(f32[512,1024]{1,0:T(8,128)S(1)} %add.61), channel_id=1, source_target_pairs={{0,4},{2,6},{4,0},{6,2},{1,5},{3,7},{5,1},{7,3},{8,12},{10,14},{12... | collective-permute-start | bytes 6291464 | tf_op jit(solution)/shard_map/ppermute | solution.py:55
Sparse Core Ops, SparseCore 0:
  156.3 164.8 all-gather.2
  368.2 66.2 all-gather.4
